TPU v7x, 32 devices: a whole 2x2x4 slice. The times are simulated.
32 devices in a mesh: tp: 8 (over z, x), dp: 4 (over y, core).
Axes of the slice: x: 2, y: 2, z: 4, core: 2. Of those that a mesh axis runs over, the one named last changes fastest.
Arguments:
- tokens: bfloat16 [128, 4096], P('tp', 'dp'), may hold values from -6 to 6
- query_weight: bfloat16 [2, 4096, 2048], P(None, 'dp', 'tp'), may hold values from -0.09375 to 0.09375
- key_weight: bfloat16 [2, 4096, 2048], P(None, 'dp', 'tp'), may hold values from -0.09375 to 0.09375
- value_weight: bfloat16 [2, 4096, 2048], P(None, 'dp', 'tp'), may hold values from -0.09375 to 0.09375
- outgate_weight: bfloat16 [2, 4096, 2048], P(None, 'dp', 'tp'), may hold values from -0.09375 to 0.09375
- igate_weight: bfloat16 [2, 4096, 16], replicated, may hold values from -0.09375 to 0.09375
- fgate_weight: bfloat16 [2, 4096, 16], replicated, may hold values from -0.09375 to 0.09375
- norm_gain: float32 [2, 4096], P(None, 'dp'), may hold values from 0.1 to 1.9
- head_gain: float32 [2, 2048], P(None, 'tp'), may hold values from 0.1 to 1.9
- proj_weight: bfloat16 [2, 2048, 4096], P(None, 'tp', 'dp'), may hold values from -0.125 to 0.125
- cell_state: float32 [2, 128, 16, 128, 128], P(None, 'dp', 'tp'), may hold values from -1.8 to 1.8
- normer_state: float32 [2, 128, 16, 128], P(None, 'dp', 'tp'), may hold values from -1.8 to 1.8
- stab_state: float32 [2, 128, 16], P(None, 'dp', 'tp'), may hold values from -4 to 4
Outputs:
- final_rows: bfloat16 [128, 4096], P('tp', 'dp')
- cell_out: float32 [2, 128, 16, 128, 128], P(None, 'dp', 'tp')
- normer_out: float32 [2, 128, 16, 128], P(None, 'dp', 'tp')
- stab_out: float32 [2, 128, 16], P(None, 'dp', 'tp')
All inputs are finite; a program needn't handle non-finite values.
Results may differ from a plain program's by a relative error of at most 0.012.
The roundings to bfloat16 on the way count: a program that leaves them out, or rounds other values in their place, can miss the bound.
Values may be sent and summed in bfloat16 or wider, within the bound.
No kernel may reach another device: no remote copies, remote signals or barrier semaphores. Data moves between devices by JAX's collectives and lax.ppermute only.
A program may use at most 64 MiB of HBM per device.

v0:
```python
import jax
import jax.numpy as jnp
from jax import lax
from jax.sharding import PartitionSpec as P

D = 4096
EPSILON = 1e-06


def gather_rows(block_input):
    return lax.all_gather(block_input, "tp", axis=0, tiled=True)


def spread_heads(out_part):
    return lax.psum_scatter(out_part, "tp", scatter_dimension=0, tiled=True)


def per_device(
    tokens,
    query_weight,
    key_weight,
    value_weight,
    outgate_weight,
    igate_weight,
    fgate_weight,
    norm_gain,
    head_gain,
    proj_weight,
    cell_state,
    normer_state,
    stab_state,
):
    dp_rank = lax.axis_index("dp")
    tp_rank = lax.axis_index("tp")
    local_seqs = cell_state.shape[1]
    local_heads = cell_state.shape[2]
    head_dim = cell_state.shape[3]
    row_width = query_weight.shape[1]
    num_blocks = query_weight.shape[0]
    gathered = gather_rows(tokens)
    final_rows = tokens
    cell_list = []
    normer_list = []
    stab_list = []
    for layer_num in range(num_blocks):
        as_float = gathered.astype(jnp.float32)
        part_squares = jnp.sum(as_float * as_float, axis=1)
        scaled = (as_float * norm_gain[layer_num]).astype(jnp.bfloat16)

        def product(weight):
            return jnp.dot(scaled, weight, preferred_element_type=jnp.float32)

        gate_start = (dp_rank * row_width, tp_rank * local_heads)
        igate_rows = lax.dynamic_slice(
            igate_weight[layer_num], gate_start, (row_width, local_heads)
        )
        fgate_rows = lax.dynamic_slice(
            fgate_weight[layer_num], gate_start, (row_width, local_heads)
        )
        query_part = product(query_weight[layer_num])
        key_part = product(key_weight[layer_num])
        value_part = product(value_weight[layer_num])
        outgate_part = product(outgate_weight[layer_num])
        igate_part = product(igate_rows)
        forget_part = product(fgate_rows)
        query_sum, key_sum, value_sum, outgate_sum, igate_sum, forget_sum = (
            lax.psum_scatter(query_part, "dp", scatter_dimension=0, tiled=True),
            lax.psum_scatter(key_part, "dp", scatter_dimension=0, tiled=True),
            lax.psum_scatter(value_part, "dp", scatter_dimension=0, tiled=True),
            lax.psum_scatter(outgate_part, "dp", scatter_dimension=0, tiled=True),
            lax.psum_scatter(igate_part, "dp", scatter_dimension=0, tiled=True),
            lax.psum_scatter(forget_part, "dp", scatter_dimension=0, tiled=True),
        )
        total_sq = lax.psum(part_squares, "dp")
        own_sq = lax.dynamic_slice_in_dim(total_sq, dp_rank * local_seqs, local_seqs)
        inv_rms = lax.rsqrt(own_sq / D + EPSILON)[:, None]
        query_rows = (query_sum * inv_rms).reshape(local_seqs, local_heads, head_dim)
        key_rows = (key_sum * inv_rms * head_dim ** (-0.5)).reshape(
            local_seqs, local_heads, head_dim
        )
        value_rows = (value_sum * inv_rms).reshape(local_seqs, local_heads, head_dim)
        outgate = outgate_sum * inv_rms
        igate = igate_sum * inv_rms
        forget = jax.nn.log_sigmoid(forget_sum * inv_rms)
        prev_stab = stab_state[layer_num]
        new_stab = jnp.maximum(forget + prev_stab, igate)
        keep_rate = jnp.exp(forget + prev_stab - new_stab)
        write_rate = jnp.exp(igate - new_stab)
        new_cell = (
            keep_rate[..., None, None] * cell_state[layer_num]
            + write_rate[..., None, None] * value_rows[..., :, None] * key_rows[..., None, :]
        )
        new_normer = (
            keep_rate[..., None] * normer_state[layer_num] + write_rate[..., None] * key_rows
        )
        numerator = jnp.einsum(
            "bhvd,bhd->bhv", new_cell, query_rows, precision=lax.Precision.HIGHEST
        )
        denominator = jnp.maximum(jnp.abs(jnp.sum(new_normer * query_rows, axis=-1)), 1.0)
        readout = numerator / denominator[..., None]
        normed = readout * lax.rsqrt(jnp.mean(readout * readout, axis=-1, keepdims=True) + EPSILON)
        normed = normed * head_gain[layer_num].reshape(local_heads, head_dim)
        gated_out = (
            jax.nn.sigmoid(outgate) * normed.reshape(local_seqs, local_heads * head_dim)
        ).astype(jnp.bfloat16)
        all_gated = lax.all_gather(gated_out, "dp", axis=0, tiled=True)
        out_part = jnp.dot(all_gated, proj_weight[layer_num], preferred_element_type=jnp.float32)
        if layer_num + 1 < num_blocks:
            gathered = lax.psum(out_part, "tp").astype(jnp.bfloat16)
        else:
            final_rows = spread_heads(out_part).astype(jnp.bfloat16)
        cell_list.append(new_cell)
        normer_list.append(new_normer)
        stab_list.append(new_stab)
    return (final_rows, jnp.stack(cell_list), jnp.stack(normer_list), jnp.stack(stab_list))


def solution(mesh):
    return jax.shard_map(
        per_device,
        mesh=mesh,
        in_specs=(
            P("tp", "dp"),
            P(None, "dp", "tp"),
            P(None, "dp", "tp"),
            P(None, "dp", "tp"),
            P(None, "dp", "tp"),
            P(),
            P(),
            P(None, "dp"),
            P(None, "tp"),
            P(None, "tp", "dp"),
            P(None, "dp", "tp", None, None),
            P(None, "dp", "tp", None),
            P(None, "dp", "tp"),
        ),
        out_specs=(
            P("tp", "dp"),
            P(None, "dp", "tp", None, None),
            P(None, "dp", "tp", None),
            P(None, "dp", "tp"),
        ),
        check_vma=False,
    )
```

profile of v0, /device:TPU:0, one launch (start us, length us, event | category | flops | bytes accessed | tf_op | source)
XLA Modules:
  0.0 431.7 jit_solution(14644992044606748619)
XLA Ops:
  7.3 0.9 fusion.90
  8.1 32.8 %all_gather.9 = bf16[128,1024]{1,0:T(8,128)(2,1)S(1)} all-gather(bf16[16,1024]{1,0:T(8,128)(2,1)} %param.13), channel_id=1, replica_groups=mesh['tp'=8,'dp'=4] {'tp'}, dimensions={0}, use_global_device_ids=true | all-gather | bytes 294912 | tf_op jit(solution)/shard_map/all_gather | solution.py:11
  40.9 1.6 fusion.89
  42.5 0.9 fusion.53
  43.5 1.6 fusion.88
  45.2 0.9 fusion.55
  46.1 1.9 fusion.36
  48.1 1.9 fusion.34
  50.2 0.9 fusion.32
  51.1 0.9 fusion.38
  52.3 5.7 %psum.21 = f32[128]{0:T(128)S(1)} all-reduce(f32[128]{0:T(128)S(1)} %fusion.17), channel_id=1, replica_groups=mesh['tp'=8,'dp'=4] {'dp'}, use_global_device_ids=true, to_apply=%region_2.0 | all-reduce | flops 128 | bytes 1024 | tf_op jit(solution)/shard_map/psum | solution.py:74
  58.0 6.2 %reduce-scatter.42.cloned.1.call-done = f32[32,2]{1,0:T(8,128)} async-done(((f32[128,2]{1,0:T(8,128)}), f32[32,2]{1,0:T(8,128)}) %reduce-scatter.42.cloned.1.call-update) | async-done | bytes 272
  64.2 0.8 copy.48
  65.0 21.2 %reduce-scatter.40.cloned.1.call-done = f32[32,2]{1,0:T(8,128)} async-done(((f32[128,2]{1,0:T(8,128)}), f32[32,2]{1,0:T(8,128)}) %reduce-scatter.40.cloned.1.call-update) | async-done | bytes 272
  86.2 0.8 copy.46
  87.2 21.6 %reduce-scatter.24.cloned.1.call-done = f32[32,256]{1,0:T(8,128)} async-done(((f32[128,256]{1,0:T(8,128)}), f32[32,256]{1,0:T(8,128)}) %reduce-scatter.24.cloned.1.call-update) | async-done | bytes 32784 | tf_op jit(solution)/shard_map/reduce_scatter | solution.py:69
  108.9 21.9 %reduce-scatter.26.cloned.1.call-done = f32[32,256]{1,0:T(8,128)} async-done(((f32[128,256]{1,0:T(8,128)}), f32[32,256]{1,0:T(8,128)}) %reduce-scatter.26.cloned.1.call-update) | async-done | bytes 32784 | tf_op jit(solution)/shard_map/reduce_scatter | solution.py:68
  130.8 21.9 %reduce-scatter.28.cloned.1.call-done = f32[32,256]{1,0:T(8,128)} async-done(((f32[128,256]{1,0:T(8,128)}), f32[32,256]{1,0:T(8,128)}) %reduce-scatter.28.cloned.1.call-update) | async-done | bytes 32784 | tf_op jit(solution)/shard_map/reduce_scatter | solution.py:67
  152.7 0.9 broadcast_multiply_fusion.5
  153.9 8.6 %fusion.4 = f32[32,2,1,128]{3,2,1,0:T(1,128)S(1)} fusion(f32[32,2,128,1]{2,3,1,0:T(1,128)S(1)} %bitcast.116, f32[2,32,2,128,128]{4,3,2,1,0:T(8,128)} %param.23, f32[32,2,128]{2,1,0:T(2,128)S(1)} %mul.366, f32[32,2,128]{2,1,0:T(2,128)S(1)} %get-tuple-element.25, f32[32,2]{1,0:T(8,128)S(1)} %copy.29), kind=kOutput, calls=%fused_computation.6 | convolution fusion | flops 15728640 | bytes 4325632 | tf_op jit(solution)/shard_map/bhvd,bhd->bhv/dot_general | solution.py:96
  162.8 11.8 %reduce-scatter.22.cloned.1.call-done = f32[32,256]{1,0:T(8,128)} async-done(((f32[128,256]{1,0:T(8,128)}), f32[32,256]{1,0:T(8,128)}) %reduce-scatter.22.cloned.1.call-update) | async-done | bytes 32784 | tf_op jit(solution)/shard_map/reduce_scatter | solution.py:70
  174.6 0.8 fusion.59
  175.5 5.2 %all_gather.10 = bf16[128,256]{1,0:T(8,128)(2,1)S(1)} all-gather(bf16[32,256]{1,0:T(8,128)(2,1)S(1)} %fusion.59), channel_id=1, replica_groups=mesh['tp'=8,'dp'=4] {'dp'}, dimensions={0}, use_global_device_ids=true | all-gather | bytes 81920 | tf_op jit(solution)/shard_map/all_gather | solution.py:106
  181.0 43.3 %all-reduce.1 = bf16[128,1024]{1,0:T(8,128)(2,1)S(1)} all-reduce(f32[128,1024]{1,0:T(8,128)S(1)} %fusion.30), channel_id=1, replica_groups=mesh['tp'=8,'dp'=4] {'tp'}, use_global_device_ids=true, to_apply=%region_10.11 | all-reduce | flops 131072 | bytes 786432 | tf_op jit(solution)/shard_map/psum | solution.py:109
  224.4 1.6 fusion.68
  226.1 1.6 fusion.66
  227.8 0.9 fusion.22
  228.7 1.9 fusion.24
  230.8 6.0 %psum.23 = f32[128]{0:T(128)S(1)} all-reduce(f32[128]{0:T(128)S(1)} %get-tuple-element.18), channel_id=1, replica_groups=mesh['tp'=8,'dp'=4] {'dp'}, use_global_device_ids=true, to_apply=%region_13.14 | all-reduce | flops 128 | bytes 1024 | tf_op jit(solution)/shard_map/psum | solution.py:74
  236.8 1.9 fusion.26
  238.9 1.9 fusion.28
  240.9 1.3 reduce-scatter.44.cloned.1.call-done
  242.2 0.8 copy.50
  243.0 21.7 %reduce-scatter.46.cloned.1.call-done = f32[32,2]{1,0:T(8,128)} async-done(((f32[128,2]{1,0:T(8,128)}), f32[32,2]{1,0:T(8,128)}) %reduce-scatter.46.cloned.1.call-update) | async-done | bytes 272
  264.7 0.8 copy.52
  266.3 20.5 %reduce-scatter.36.cloned.1.call-done = f32[32,256]{1,0:T(8,128)} async-done(((f32[128,256]{1,0:T(8,128)}), f32[32,256]{1,0:T(8,128)}) %reduce-scatter.36.cloned.1.call-update) | async-done | bytes 32784 | tf_op jit(solution)/shard_map/reduce_scatter | solution.py:67
  286.8 21.9 %reduce-scatter.34.cloned.1.call-done = f32[32,256]{1,0:T(8,128)} async-done(((f32[128,256]{1,0:T(8,128)}), f32[32,256]{1,0:T(8,128)}) %reduce-scatter.34.cloned.1.call-update) | async-done | bytes 32784 | tf_op jit(solution)/shard_map/reduce_scatter | solution.py:68
  308.7 22.7 %reduce-scatter.32.cloned.1.call-done = f32[32,256]{1,0:T(8,128)} async-done(((f32[128,256]{1,0:T(8,128)}), f32[32,256]{1,0:T(8,128)}) %reduce-scatter.32.cloned.1.call-update) | async-done | bytes 32784 | tf_op jit(solution)/shard_map/reduce_scatter | solution.py:69
  331.4 0.9 broadcast_multiply_fusion.2
  332.6 8.6 %fusion.1 = f32[32,2,1,128]{3,2,1,0:T(1,128)S(1)} fusion(f32[32,2,128,1]{2,3,1,0:T(1,128)S(1)} %bitcast.117, f32[2,32,2,128,128]{4,3,2,1,0:T(8,128)} %param.23, f32[32,2,128]{2,1,0:T(2,128)S(1)} %mul.398, f32[32,2,128]{2,1,0:T(2,128)S(1)} %get-tuple-element.23, f32[32,2]{1,0:T(8,128)S(1)} %copy.32), kind=kOutput, calls=%fused_computation.3 | convolution fusion | flops 15728640 | bytes 4325632 | tf_op jit(solution)/shard_map/bhvd,bhd->bhv/dot_general | solution.py:96
  341.5 11.8 %reduce-scatter.30.cloned.1.call-done = f32[32,256]{1,0:T(8,128)} async-done(((f32[128,256]{1,0:T(8,128)}), f32[32,256]{1,0:T(8,128)}) %reduce-scatter.30.cloned.1.call-update) | async-done | bytes 32784 | tf_op jit(solution)/shard_map/reduce_scatter | solution.py:70
  353.3 0.8 fusion.58
  354.1 5.2 %all_gather.11 = bf16[128,256]{1,0:T(8,128)(2,1)S(1)} all-gather(bf16[32,256]{1,0:T(8,128)(2,1)S(1)} %fusion.58), channel_id=1, replica_groups=mesh['tp'=8,'dp'=4] {'dp'}, dimensions={0}, use_global_device_ids=true | all-gather | bytes 81920 | tf_op jit(solution)/shard_map/all_gather | solution.py:106
  359.4 1.0 fusion.20
  361.3 5.4 %multiply_add_fusion.1 = (f32[1,32,2,128,128]{4,3,2,1,0:T(8,128)S(1)}, f32[1,32,2,128,128]{4,3,2,1,0:T(8,128)S(1)}) fusion(f32[2,32,2,128,128]{4,3,2,1,0:T(8,128)} %param.23, f32[32,2,128]{2,1,0:T(2,128)S(1)} %mul.366, f32[32,2,128]{2,1,0:T(2,128)S(1)} %get-tuple-element.25, f32[32,2]{1,0:T(8,128)S(1)} %copy.29, f32[32,2,128]{2,1,0:T(2,128)S(1)} %mul.398, ...), kind=kLoop, calls=%fused_computation.8 | loop fusion | flops 6291456 | bytes 16908800 | tf_op jit(solution)/shard_map/add | solution.py:90
  366.7 4.0 pad_maximum_fusion
  370.7 53.0 %reduce-scatter.38.cloned.1.call-done = f32[16,1024]{1,0:T(8,128)} async-done(((f32[128,1024]{1,0:T(8,128)}), f32[16,1024]{1,0:T(8,128)}) %reduce-scatter.38.cloned.1.call-update) | async-done | bytes 65552 | tf_op jit(solution)/shard_map/reduce_scatter | solution.py:15
  423.7 1.5 convert_element_type.31
  (75 shorter events, 4.6 us)
Async XLA Ops:
  7.2 43.0 %copy-start.1 = (bf16[2,1024,256]{2,1,0:T(8,128)(2,1)S(1)}, bf16[2,1024,256]{2,1,0:T(8,128)(2,1)}, u32[]{:S(2)}) copy-start(bf16[2,1024,256]{2,1,0:T(8,128)(2,1)} %param.14) | copy-start | bytes 3145732
  7.2 44.0 %copy-start.2 = (bf16[2,1024,256]{2,1,0:T(8,128)(2,1)S(1)}, bf16[2,1024,256]{2,1,0:T(8,128)(2,1)}, u32[]{:S(2)}) copy-start(bf16[2,1024,256]{2,1,0:T(8,128)(2,1)} %param.17) | copy-start | bytes 3145732
  7.2 45.1 %copy-start.4 = (f32[2,256]{1,0:T(2,128)S(1)}, f32[2,256]{1,0:T(2,128)}, u32[]{:S(2)}) copy-start(f32[2,256]{1,0:T(2,128)} %param.21) | copy-start | bytes 6148
  7.2 79.8 %copy-start.5 = (f32[2,32,2]{1,2,0:T(2,128)S(1)}, f32[2,32,2]{1,2,0:T(2,128)}, u32[]{:S(2)}) copy-start(f32[2,32,2]{1,2,0:T(2,128)} %param.25) | copy-start | bytes 1540
  7.2 146.5 %copy-start.3 = (f32[2,32,2,128]{3,2,1,0:T(2,128)S(1)}, f32[2,32,2,128]{3,2,1,0:T(2,128)}, u32[]{:S(2)}) copy-start(f32[2,32,2,128]{3,2,1,0:T(2,128)} %param.24) | copy-start | bytes 196612
  7.2 57.0 %reduce-scatter.42.cloned.1.call-start = ((), (), s32[]{:S(2)}) async-start(), calls=%async_computation.23 | async-start | bytes 81920
  43.5 42.7 %reduce-scatter.40.cloned.1.call-start = ((), (), s32[]{:S(2)}) async-start(), calls=%async_computation.22 | async-start | bytes 81920
  46.1 62.8 %reduce-scatter.24.cloned.1.call-start = ((), (), s32[]{:S(2)}) async-start(), calls=%async_computation.14 | async-start | bytes 163840 | tf_op jit(solution)/shard_map/reduce_scatter | solution.py:69
  48.1 82.7 %reduce-scatter.26.cloned.1.call-start = ((), (), s32[]{:S(2)}) async-start(), calls=%async_computation.15 | async-start | bytes 163840 | tf_op jit(solution)/shard_map/reduce_scatter | solution.py:68
  50.1 102.6 %reduce-scatter.28.cloned.1.call-start = ((), (), s32[]{:S(2)}) async-start(), calls=%async_computation.16 | async-start | bytes 163840 | tf_op jit(solution)/shard_map/reduce_scatter | solution.py:67
  51.0 129.7 %copy-start = (bf16[2,256,1024]{2,1,0:T(8,128)(2,1)S(1)}, bf16[2,256,1024]{2,1,0:T(8,128)(2,1)}, u32[]{:S(2)}) copy-start(bf16[2,256,1024]{2,1,0:T(8,128)(2,1)} %param.22) | copy-start | bytes 3145732
  51.1 123.6 %reduce-scatter.22.cloned.1.call-start = ((), (), s32[]{:S(2)}) async-start(), calls=%async_computation.13 | async-start | bytes 163840 | tf_op jit(solution)/shard_map/reduce_scatter | solution.py:70
  52.1 190.1 %reduce-scatter.44.cloned.1.call-start = ((), (), s32[]{:S(2)}) async-start(), calls=%async_computation.24 | async-start | bytes 81920
  226.0 38.6 %reduce-scatter.46.cloned.1.call-start = ((), (), s32[]{:S(2)}) async-start(), calls=%async_computation.25 | async-start | bytes 81920
  227.7 59.0 %reduce-scatter.36.cloned.1.call-start = ((), (), s32[]{:S(2)}) async-start(), calls=%async_computation.20 | async-start | bytes 163840 | tf_op jit(solution)/shard_map/reduce_scatter | solution.py:67
  228.7 80.0 %reduce-scatter.34.cloned.1.call-start = ((), (), s32[]{:S(2)}) async-start(), calls=%async_computation.19 | async-start | bytes 163840 | tf_op jit(solution)/shard_map/reduce_scatter | solution.py:68
  230.7 100.7 %reduce-scatter.32.cloned.1.call-start = ((), (), s32[]{:S(2)}) async-start(), calls=%async_computation.18 | async-start | bytes 163840 | tf_op jit(solution)/shard_map/reduce_scatter | solution.py:69
  238.7 114.6 %reduce-scatter.30.cloned.1.call-start = ((), (), s32[]{:S(2)}) async-start(), calls=%async_computation.17 | async-start | bytes 163840 | tf_op jit(solution)/shard_map/reduce_scatter | solution.py:70
  240.8 182.8 %reduce-scatter.38.cloned.1.call-start = ((), (), s32[]{:S(2)}) async-start(), calls=%async_computation.21 | async-start | bytes 589824 | tf_op jit(solution)/shard_map/reduce_scatter | solution.py:15
Sparse Core Ops, SparseCore 0:
  43.6 20.5 reduce-scatter.41
  66.6 19.5 reduce-scatter.39
  89.2 19.6 reduce-scatter.23
  111.1 19.6 reduce-scatter.25
  133.1 19.6 reduce-scatter.27
  155.0 19.6 reduce-scatter.21
  226.2 15.9 reduce-scatter.43
  245.1 19.4 reduce-scatter.45
  267.1 19.6 reduce-scatter.35
  289.1 19.6 reduce-scatter.33
  311.7 19.6 reduce-scatter.31
  333.6 19.6 reduce-scatter.29
  360.6 63.0 reduce-scatter.37
where the time goes:
time: 433 us; the launch traced here: 432 us
  waiting for transfers between devices  258 us (60%)
  blocking collectives  98.2 us (23%)
  matrix products  35.8 us (8%)
  other arithmetic  17.3 us (4%)
  between operations  14.2 us (3%)
  local copies, waits for them, and re-layouts  7.86 us (2%)
    reduce_scatter x1, waiting for transfers between devices, spread_heads(): return lax.psum_scatter(out_part, 'tp', scatter_dimension=0, tiled=True)  53 us
    unnamed x17, waiting for transfers between devices  50.6 us
    reduce_scatter x2, waiting for transfers between devices, per_device(): lax.psum_scatter(value_part, 'dp', scatter_dimension=0, tiled=True)  44.3 us
    reduce_scatter x2, waiting for transfers between devices, per_device(): lax.psum_scatter(key_part, 'dp', scatter_dimension=0, tiled=True)  43.9 us
    psum x1, blocking collectives, per_device(): gathered = lax.psum(out_part, 'tp').astype(jnp.bfloat16)  43.3 us
    reduce_scatter x2, waiting for transfers between devices, per_device(): lax.psum_scatter(query_part, 'dp', scatter_dimension=0, tiled=True)  42.4 us
    all_gather x1, blocking collectives, gather_rows(): return lax.all_gather(block_input, 'tp', axis=0, tiled=True)  32.8 us
    reduce_scatter x2, waiting for transfers between devices, per_device(): lax.psum_scatter(outgate_part, 'dp', scatter_dimension=0, tiled=True)  23.6 us
  transfers between devices with their start and end apart: 13, of which 13 were waited for; matrix products, arithmetic and copies ran while one was open for 12% of the time, Pallas kernels for 0%

commit v1 on v0

--- a/solution.py
+++ b/solution.py
@@ -106,7 +106,7 @@
         all_gated = lax.all_gather(gated_out, "dp", axis=0, tiled=True)
         out_part = jnp.dot(all_gated, proj_weight[layer_num], preferred_element_type=jnp.float32)
         if layer_num + 1 < num_blocks:
-            gathered = lax.psum(out_part, "tp").astype(jnp.bfloat16)
+            gathered = jnp.sum(lax.all_gather(out_part, "tp"), axis=0).astype(jnp.bfloat16)
         else:
             final_rows = spread_heads(out_part).astype(jnp.bfloat16)
         cell_list.append(new_cell)

time: 433 us -> 468 us (1.081)
  waiting for transfers between devices: 258 us -> 333 us
  blocking collectives: 98.2 us -> 54.6 us
    all_gather x0 -> x1, waiting for transfers between devices: none -> 72.9 us  [per_device(): lax.all_gather(out_part, 'tp')]
    psum x1 -> x0, blocking collectives: 43.3 us -> none  [per_device(): gathered = lax.psum(out_part, 'tp').astype(jnp.bfloat16)]
    unnamed x17 -> x18, waiting for transfers between devices: 50.6 us -> 53.2 us
  transfers between devices with their start and end apart: 13 -> 14, of which waited for: 13 -> 14; matrix products, arithmetic and copies ran while one was open for 12% -> 11% of each run, Pallas kernels for 0% -> 0%
where the time goes in v1:
time: 468 us; the launch traced here: 467 us
  waiting for transfers between devices  333 us (71%)
  blocking collectives  54.6 us (12%)
  matrix products  36.6 us (8%)
  other arithmetic  19.9 us (4%)
  between operations  14.2 us (3%)
  local copies, waits for them, and re-layouts  7.86 us (2%)
    all_gather x1, waiting for transfers between devices, per_device(): lax.all_gather(out_part, 'tp')  72.9 us
    unnamed x18, waiting for transfers between devices  53.2 us
    reduce_scatter x1, waiting for transfers between devices, spread_heads(): return lax.psum_scatter(out_part, 'tp', scatter_dimension=0, tiled=True)  53 us
    reduce_scatter x2, waiting for transfers between devices, per_device(): lax.psum_scatter(value_part, 'dp', scatter_dimension=0, tiled=True)  44.2 us
    reduce_scatter x2, waiting for transfers between devices, per_device(): lax.psum_scatter(key_part, 'dp', scatter_dimension=0, tiled=True)  44.1 us
    reduce_scatter x2, waiting for transfers between devices, per_device(): lax.psum_scatter(query_part, 'dp', scatter_dimension=0, tiled=True)  42.3 us
    all_gather x1, blocking collectives, gather_rows(): return lax.all_gather(block_input, 'tp', axis=0, tiled=True)  32.8 us
    reduce_scatter x2, waiting for transfers between devices, per_device(): lax.psum_scatter(outgate_part, 'dp', scatter_dimension=0, tiled=True)  23.8 us
  transfers between devices with their start and end apart: 14, of which 14 were waited for; matrix products, arithmetic and copies ran while one was open for 11% of the time, Pallas kernels for 0%

profile of v1, /device:TPU:0, one launch (start us, length us, event | category | flops | bytes accessed | tf_op | source)
XLA Modules:
  0.0 467.1 jit_solution(6951650770260440371)
XLA Ops:
  7.3 0.9 fusion.90
  8.1 32.8 %all_gather.15 = bf16[128,1024]{1,0:T(8,128)(2,1)S(1)} all-gather(bf16[16,1024]{1,0:T(8,128)(2,1)} %param.13), channel_id=1, replica_groups=mesh['tp'=8,'dp'=4] {'tp'}, dimensions={0}, use_global_device_ids=true | all-gather | bytes 294912 | tf_op jit(solution)/shard_map/all_gather | solution.py:11
  40.9 1.6 fusion.89
  42.5 0.9 fusion.53
  43.5 1.6 fusion.88
  45.1 0.9 fusion.55
  46.1 1.9 fusion.36
  48.1 1.9 fusion.34
  50.2 0.9 fusion.32
  51.1 0.9 fusion.38
  52.2 5.7 %psum.14 = f32[128]{0:T(128)S(1)} all-reduce(f32[128]{0:T(128)S(1)} %fusion.17), channel_id=1, replica_groups=mesh['tp'=8,'dp'=4] {'dp'}, use_global_device_ids=true, to_apply=%region_2.0 | all-reduce | flops 128 | bytes 1024 | tf_op jit(solution)/shard_map/psum | solution.py:74
  58.0 6.2 %reduce-scatter.42.cloned.1.call-done = f32[32,2]{1,0:T(8,128)} async-done(((f32[128,2]{1,0:T(8,128)}), f32[32,2]{1,0:T(8,128)}) %reduce-scatter.42.cloned.1.call-update) | async-done | bytes 272
  64.2 0.8 copy.60
  65.0 21.2 %reduce-scatter.40.cloned.1.call-done = f32[32,2]{1,0:T(8,128)} async-done(((f32[128,2]{1,0:T(8,128)}), f32[32,2]{1,0:T(8,128)}) %reduce-scatter.40.cloned.1.call-update) | async-done | bytes 272
  87.2 21.7 %reduce-scatter.24.cloned.1.call-done = f32[32,256]{1,0:T(8,128)} async-done(((f32[128,256]{1,0:T(8,128)}), f32[32,256]{1,0:T(8,128)}) %reduce-scatter.24.cloned.1.call-update) | async-done | bytes 32784 | tf_op jit(solution)/shard_map/reduce_scatter | solution.py:69
  108.9 22.0 %reduce-scatter.26.cloned.1.call-done = f32[32,256]{1,0:T(8,128)} async-done(((f32[128,256]{1,0:T(8,128)}), f32[32,256]{1,0:T(8,128)}) %reduce-scatter.26.cloned.1.call-update) | async-done | bytes 32784 | tf_op jit(solution)/shard_map/reduce_scatter | solution.py:68
  130.9 22.0 %reduce-scatter.28.cloned.1.call-done = f32[32,256]{1,0:T(8,128)} async-done(((f32[128,256]{1,0:T(8,128)}), f32[32,256]{1,0:T(8,128)}) %reduce-scatter.28.cloned.1.call-update) | async-done | bytes 32784 | tf_op jit(solution)/shard_map/reduce_scatter | solution.py:67
  152.8 0.9 broadcast_multiply_fusion.5
  154.0 8.6 %fusion.4 = f32[32,2,1,128]{3,2,1,0:T(1,128)S(1)} fusion(f32[32,2,128,1]{2,3,1,0:T(1,128)S(1)} %bitcast.118, f32[2,32,2,128,128]{4,3,2,1,0:T(8,128)} %param.23, f32[32,2,128]{2,1,0:T(2,128)S(1)} %mul.366, f32[32,2,128]{2,1,0:T(2,128)S(1)} %get-tuple-element.25, f32[32,2]{1,0:T(8,128)S(1)} %copy.41), kind=kOutput, calls=%fused_computation.6 | convolution fusion | flops 15728640 | bytes 4325632 | tf_op jit(solution)/shard_map/bhvd,bhd->bhv/dot_general | solution.py:96
  163.0 11.8 %reduce-scatter.22.cloned.1.call-done = f32[32,256]{1,0:T(8,128)} async-done(((f32[128,256]{1,0:T(8,128)}), f32[32,256]{1,0:T(8,128)}) %reduce-scatter.22.cloned.1.call-update) | async-done | bytes 32784 | tf_op jit(solution)/shard_map/reduce_scatter | solution.py:70
  174.8 0.8 fusion.59
  175.6 5.2 %all_gather.16 = bf16[128,256]{1,0:T(8,128)(2,1)S(1)} all-gather(bf16[32,256]{1,0:T(8,128)(2,1)S(1)} %fusion.59), channel_id=1, replica_groups=mesh['tp'=8,'dp'=4] {'dp'}, dimensions={0}, use_global_device_ids=true | all-gather | bytes 81920 | tf_op jit(solution)/shard_map/all_gather | solution.py:106
  180.9 1.0 fusion.30
  182.0 72.9 %all-gather.3.cloned.1.call-done = f32[1024,1024]{1,0:T(8,128)} async-done(((f32[128,1024]{1,0:T(8,128)}), f32[1024,1024]{1,0:T(8,128)}) %all-gather.3.cloned.1.call-update) | async-done | bytes 4194320 | tf_op jit(solution)/shard_map/all_gather | solution.py:109
  254.9 2.6 reduce_sum.66
  257.7 1.6 fusion.68
  259.4 1.6 fusion.66
  261.1 0.9 fusion.22
  262.0 1.9 fusion.24
  264.1 5.7 %psum.15 = f32[128]{0:T(128)S(1)} all-reduce(f32[128]{0:T(128)S(1)} %get-tuple-element.18), channel_id=1, replica_groups=mesh['tp'=8,'dp'=4] {'dp'}, use_global_device_ids=true, to_apply=%region_13.14 | all-reduce | flops 128 | bytes 1024 | tf_op jit(solution)/shard_map/psum | solution.py:74
  269.7 1.9 fusion.26
  271.8 1.9 fusion.28
  273.8 3.7 reduce-scatter.44.cloned.1.call-done
  277.5 0.8 copy.62
  278.3 21.8 %reduce-scatter.46.cloned.1.call-done = f32[32,2]{1,0:T(8,128)} async-done(((f32[128,2]{1,0:T(8,128)}), f32[32,2]{1,0:T(8,128)}) %reduce-scatter.46.cloned.1.call-update) | async-done | bytes 272
  301.7 20.4 %reduce-scatter.36.cloned.1.call-done = f32[32,256]{1,0:T(8,128)} async-done(((f32[128,256]{1,0:T(8,128)}), f32[32,256]{1,0:T(8,128)}) %reduce-scatter.36.cloned.1.call-update) | async-done | bytes 32784 | tf_op jit(solution)/shard_map/reduce_scatter | solution.py:67
  322.1 22.1 %reduce-scatter.34.cloned.1.call-done = f32[32,256]{1,0:T(8,128)} async-done(((f32[128,256]{1,0:T(8,128)}), f32[32,256]{1,0:T(8,128)}) %reduce-scatter.34.cloned.1.call-update) | async-done | bytes 32784 | tf_op jit(solution)/shard_map/reduce_scatter | solution.py:68
  344.2 22.5 %reduce-scatter.32.cloned.1.call-done = f32[32,256]{1,0:T(8,128)} async-done(((f32[128,256]{1,0:T(8,128)}), f32[32,256]{1,0:T(8,128)}) %reduce-scatter.32.cloned.1.call-update) | async-done | bytes 32784 | tf_op jit(solution)/shard_map/reduce_scatter | solution.py:69
  366.7 0.9 broadcast_multiply_fusion.2
  367.9 8.6 %fusion.1 = f32[32,2,1,128]{3,2,1,0:T(1,128)S(1)} fusion(f32[32,2,128,1]{2,3,1,0:T(1,128)S(1)} %bitcast.119, f32[2,32,2,128,128]{4,3,2,1,0:T(8,128)} %param.23, f32[32,2,128]{2,1,0:T(2,128)S(1)} %mul.398, f32[32,2,128]{2,1,0:T(2,128)S(1)} %get-tuple-element.23, f32[32,2]{1,0:T(8,128)S(1)} %copy.44), kind=kOutput, calls=%fused_computation.3 | convolution fusion | flops 15728640 | bytes 4325632 | tf_op jit(solution)/shard_map/bhvd,bhd->bhv/dot_general | solution.py:96
  376.8 11.9 %reduce-scatter.30.cloned.1.call-done = f32[32,256]{1,0:T(8,128)} async-done(((f32[128,256]{1,0:T(8,128)}), f32[32,256]{1,0:T(8,128)}) %reduce-scatter.30.cloned.1.call-update) | async-done | bytes 32784 | tf_op jit(solution)/shard_map/reduce_scatter | solution.py:70
  388.8 0.8 fusion.58
  389.6 5.2 %all_gather.19 = bf16[128,256]{1,0:T(8,128)(2,1)S(1)} all-gather(bf16[32,256]{1,0:T(8,128)(2,1)S(1)} %fusion.58), channel_id=1, replica_groups=mesh['tp'=8,'dp'=4] {'dp'}, dimensions={0}, use_global_device_ids=true | all-gather | bytes 81920 | tf_op jit(solution)/shard_map/all_gather | solution.py:106
  394.8 1.0 fusion.20
  396.8 5.4 %multiply_add_fusion.1 = (f32[1,32,2,128,128]{4,3,2,1,0:T(8,128)S(1)}, f32[1,32,2,128,128]{4,3,2,1,0:T(8,128)S(1)}) fusion(f32[2,32,2,128,128]{4,3,2,1,0:T(8,128)} %param.23, f32[32,2,128]{2,1,0:T(2,128)S(1)} %mul.366, f32[32,2,128]{2,1,0:T(2,128)S(1)} %get-tuple-element.25, f32[32,2]{1,0:T(8,128)S(1)} %copy.41, f32[32,2,128]{2,1,0:T(2,128)S(1)} %mul.398, ...), kind=kLoop, calls=%fused_computation.8 | loop fusion | flops 6291456 | bytes 16908800 | tf_op jit(solution)/shard_map/add | solution.py:90
  402.2 4.0 pad_maximum_fusion
  406.1 53.0 %reduce-scatter.38.cloned.1.call-done = f32[16,1024]{1,0:T(8,128)} async-done(((f32[128,1024]{1,0:T(8,128)}), f32[16,1024]{1,0:T(8,128)}) %reduce-scatter.38.cloned.1.call-update) | async-done | bytes 65552 | tf_op jit(solution)/shard_map/reduce_scatter | solution.py:15
  459.1 1.5 convert_element_type.31
  (78 shorter events, 6.0 us)
Async XLA Ops:
  7.2 43.0 %copy-start.1 = (bf16[2,1024,256]{2,1,0:T(8,128)(2,1)S(1)}, bf16[2,1024,256]{2,1,0:T(8,128)(2,1)}, u32[]{:S(2)}) copy-start(bf16[2,1024,256]{2,1,0:T(8,128)(2,1)} %param.14) | copy-start | bytes 3145732
  7.2 44.0 %copy-start.2 = (bf16[2,1024,256]{2,1,0:T(8,128)(2,1)S(1)}, bf16[2,1024,256]{2,1,0:T(8,128)(2,1)}, u32[]{:S(2)}) copy-start(bf16[2,1024,256]{2,1,0:T(8,128)(2,1)} %param.17) | copy-start | bytes 3145732
  7.2 45.0 %copy-start.4 = (f32[2,256]{1,0:T(2,128)S(1)}, f32[2,256]{1,0:T(2,128)}, u32[]{:S(2)}) copy-start(f32[2,256]{1,0:T(2,128)} %param.21) | copy-start | bytes 6148
  7.2 79.8 %copy-start.5 = (f32[2,32,2]{1,2,0:T(2,128)S(1)}, f32[2,32,2]{1,2,0:T(2,128)}, u32[]{:S(2)}) copy-start(f32[2,32,2]{1,2,0:T(2,128)} %param.25) | copy-start | bytes 1540
  7.2 146.6 %copy-start.3 = (f32[2,32,2,128]{3,2,1,0:T(2,128)S(1)}, f32[2,32,2,128]{3,2,1,0:T(2,128)}, u32[]{:S(2)}) copy-start(f32[2,32,2,128]{3,2,1,0:T(2,128)} %param.24) | copy-start | bytes 196612
  7.2 57.0 %reduce-scatter.42.cloned.1.call-start = ((), (), s32[]{:S(2)}) async-start(), calls=%async_computation.24 | async-start | bytes 81920
  43.5 42.7 %reduce-scatter.40.cloned.1.call-start = ((), (), s32[]{:S(2)}) async-start(), calls=%async_computation.23 | async-start | bytes 81920
  46.1 62.8 %reduce-scatter.24.cloned.1.call-start = ((), (), s32[]{:S(2)}) async-start(), calls=%async_computation.14 | async-start | bytes 163840 | tf_op jit(solution)/shard_map/reduce_scatter | solution.py:69
  48.1 82.8 %reduce-scatter.26.cloned.1.call-start = ((), (), s32[]{:S(2)}) async-start(), calls=%async_computation.15 | async-start | bytes 163840 | tf_op jit(solution)/shard_map/reduce_scatter | solution.py:68
  50.1 102.7 %reduce-scatter.28.cloned.1.call-start = ((), (), s32[]{:S(2)}) async-start(), calls=%async_computation.16 | async-start | bytes 163840 | tf_op jit(solution)/shard_map/reduce_scatter | solution.py:67
  51.0 129.8 %copy-start = (bf16[2,256,1024]{2,1,0:T(8,128)(2,1)S(1)}, bf16[2,256,1024]{2,1,0:T(8,128)(2,1)}, u32[]{:S(2)}) copy-start(bf16[2,256,1024]{2,1,0:T(8,128)(2,1)} %param.22) | copy-start | bytes 3145732
  51.1 123.7 %reduce-scatter.22.cloned.1.call-start = ((), (), s32[]{:S(2)}) async-start(), calls=%async_computation.13 | async-start | bytes 163840 | tf_op jit(solution)/shard_map/reduce_scatter | solution.py:70
  52.0 202.9 %all-gather.3.cloned.1.call-start = ((), (), s32[]{:S(2)}) async-start(), calls=%async_computation.22 | async-start | bytes 4718592 | tf_op jit(solution)/shard_map/all_gather | solution.py:109
  181.9 95.6 %reduce-scatter.44.cloned.1.call-start = ((), (), s32[]{:S(2)}) async-start(), calls=%async_computation.25 | async-start | bytes 81920
  259.3 40.8 %reduce-scatter.46.cloned.1.call-start = ((), (), s32[]{:S(2)}) async-start(), calls=%async_computation.26 | async-start | bytes 81920
  261.0 61.0 %reduce-scatter.36.cloned.1.call-start = ((), (), s32[]{:S(2)}) async-start(), calls=%async_computation.20 | async-start | bytes 163840 | tf_op jit(solution)/shard_map/reduce_scatter | solution.py:67
  262.0 82.2 %reduce-scatter.34.cloned.1.call-start = ((), (), s32[]{:S(2)}) async-start(), calls=%async_computation.19 | async-start | bytes 163840 | tf_op jit(solution)/shard_map/reduce_scatter | solution.py:68
  264.0 102.7 %reduce-scatter.32.cloned.1.call-start = ((), (), s32[]{:S(2)}) async-start(), calls=%async_computation.18 | async-start | bytes 163840 | tf_op jit(solution)/shard_map/reduce_scatter | solution.py:69
  271.7 117.1 %reduce-scatter.30.cloned.1.call-start = ((), (), s32[]{:S(2)}) async-start(), calls=%async_computation.17 | async-start | bytes 163840 | tf_op jit(solution)/shard_map/reduce_scatter | solution.py:70
  273.8 185.4 %reduce-scatter.38.cloned.1.call-start = ((), (), s32[]{:S(2)}) async-start(), calls=%async_computation.21 | async-start | bytes 589824 | tf_op jit(solution)/shard_map/reduce_scatter | solution.py:15
Sparse Core Ops, SparseCore 0:
  43.6 20.5 reduce-scatter.41
  66.6 19.5 reduce-scatter.39
  89.2 19.6 reduce-scatter.23
  111.2 19.6 reduce-scatter.25
  133.1 19.6 reduce-scatter.27
  155.1 19.6 reduce-scatter.21
  182.1 72.7 all-gather.2
  259.4 18.0 reduce-scatter.43
  280.5 19.5 reduce-scatter.45
  302.4 19.6 reduce-scatter.35
  324.5 19.6 reduce-scatter.33
  347.0 19.6 reduce-scatter.31
  369.1 19.6 reduce-scatter.29
  396.0 63.0 reduce-scatter.37
